TPU v7x, 32 devices: a whole 2x2x4 slice. The times are simulated.
32 devices in a mesh: sp: 8 (over z, core), tp: 4 (over y, x).
Axes of the slice: x: 2, y: 2, z: 4, core: 2. Of those that a mesh axis runs over, the one named last changes fastest.
Arguments:
- residual_in: bfloat16 [2048, 2048], P('sp'), may hold values from -3 to 3
- mix_gain: float32 [2048], replicated, may hold values from 0.1 to 1.9
- pool_weight: bfloat16 [512, 2048], P(None, 'tp'), may hold values from -0.5 to 0.5
- pool_scale: float32 [2048], P('tp'), may hold values from 0.1 to 1.9
- ffn_gain: float32 [2048], replicated, may hold values from 0.1 to 1.9
- route_ids: int32 [2048, 2], P('sp'), may hold values from 0 to 7, all different within a row; in each aligned block of 64 rows (0 to 63, 64 to 127, ...) at most 32 rows name the same one
- route_weights: float32 [2048, 2], P('sp'), may hold values from 0.1 to 1
- gate_weight: bfloat16 [8, 2048, 3584], P('sp', None, 'tp'), may hold values from -0.125 to 0.125
- up_weight: bfloat16 [8, 2048, 3584], P('sp', None, 'tp'), may hold values from -0.125 to 0.125
- down_weight: bfloat16 [8, 3584, 2048], P('sp', 'tp'), may hold values from -0.09375 to 0.09375
Outputs:
- layer_out: bfloat16 [2048, 2048], P('sp')
Inputs may be any that keep to these rules, and one draw needn't show every extreme that they name: `route_ids`: each row names 2 different experts; in each aligned block of 64 rows no expert is named by more than 32 rows, and some block has an expert named by exactly 32 rows.
All inputs are finite; a program needn't handle non-finite values.
Results may differ from a plain program's by a relative error of at most 0.0074.
Values may be sent and summed in bfloat16 or wider, within the bound.
A program may use at most 64 MiB of HBM per device.

v0:
```python
import jax
import jax.numpy as jnp
from jax import lax
from jax.sharding import PartitionSpec as P

GROUPS = 4
SPAN = 16
TOP_K = 2


EPS = 1e-06


def from_behind(value, axis, steps):
    count = lax.axis_size(axis)
    first, last = (max(0, -steps), min(count, count - steps))
    return lax.ppermute(value, axis, [(source, source + steps) for source in range(first, last)])


def rms_scale(values, gain):
    return values * lax.rsqrt(jnp.mean(values * values, axis=-1, keepdims=True) + EPS) * gain


def slot_table(chosen_ids, experts, capacity):
    flat_ids = chosen_ids.reshape(-1)
    matches = (flat_ids[:, None] == jnp.arange(experts, dtype=jnp.int32)[None, :]).astype(jnp.int32)
    before = jnp.cumsum(matches, axis=0) - matches
    slot_of = jnp.sum(before * matches, axis=1)
    target = flat_ids * capacity + slot_of
    return (target[:, None] == jnp.arange(experts * capacity, dtype=jnp.int32)[None, :]).astype(
        jnp.float32
    )


def shards(
    residual_in,
    mix_gain,
    pool_weight,
    pool_scale,
    ffn_gain,
    route_ids,
    route_weights,
    gate_weight,
    up_weight,
    down_weight,
):
    tp_count = lax.axis_size("tp")
    sp_count = lax.axis_size("sp")
    tp_index = lax.axis_index("tp")
    tok_count, width = residual_in.shape
    group_width = width // GROUPS
    col_count = pool_weight.shape[1]
    row_count = tok_count // tp_count
    capacity = 2 * TOP_K * row_count // sp_count
    group_index = tp_index * col_count // group_width
    window = jnp.power(2, group_index + 1)
    stream = residual_in.astype(jnp.float32)
    inverse = lax.rsqrt(jnp.mean(stream * stream, axis=-1, keepdims=True) + EPS)
    stream_group = lax.dynamic_slice_in_dim(stream, group_index * group_width, group_width, 1)
    gain_group = lax.dynamic_slice_in_dim(mix_gain, group_index * group_width, group_width, 0)
    normed_group = (stream_group * inverse * gain_group).astype(jnp.bfloat16)
    rim_rows = from_behind(normed_group[tok_count - SPAN :], "sp", 1)
    extended = jnp.concatenate([rim_rows, normed_group], axis=0).astype(jnp.float32)
    window_sum = jnp.zeros((tok_count, group_width), jnp.float32)
    for offset in range(SPAN):
        window_sum = window_sum + jnp.where(
            offset < window, extended[SPAN - offset : SPAN - offset + tok_count], 0.0
        )
    position = lax.axis_index("sp") * tok_count + jnp.arange(tok_count, dtype=jnp.int32)
    divisor = jnp.minimum(position + 1, window).astype(jnp.float32)
    pooled = (window_sum / divisor[:, None] - extended[SPAN:]).astype(jnp.bfloat16)
    mixed = (jnp.dot(pooled, pool_weight, preferred_element_type=jnp.float32) * pool_scale).astype(
        jnp.bfloat16
    )
    stream_own = lax.dynamic_slice_in_dim(stream, tp_index * row_count, row_count, 0)
    mixed_own = lax.all_to_all(mixed, "tp", split_axis=0, concat_axis=1, tiled=True)
    after_own = (stream_own + mixed_own.astype(jnp.float32)).astype(jnp.bfloat16)
    normed_own = rms_scale(after_own.astype(jnp.float32), ffn_gain).astype(jnp.bfloat16)
    ids_own = lax.dynamic_slice_in_dim(route_ids, tp_index * row_count, row_count, 0)
    table_own = slot_table(ids_own, sp_count, capacity)
    repeated = jnp.repeat(normed_own, TOP_K, axis=0)
    outgoing = lax.dot_general(
        table_own.astype(jnp.bfloat16),
        repeated,
        (((0,), (0,)), ((), ())),
        preferred_element_type=jnp.float32,
    )
    outgoing = outgoing.astype(jnp.bfloat16).reshape(sp_count, capacity, width)
    arrived = lax.all_to_all(outgoing, "sp", split_axis=0, concat_axis=0, tiled=True)
    piece = lax.all_gather(arrived, "tp", axis=0, tiled=True)
    flat_rows = piece.reshape(-1, width)
    gate_part = jnp.dot(flat_rows, gate_weight[0], preferred_element_type=jnp.float32)
    up_part = jnp.dot(flat_rows, up_weight[0], preferred_element_type=jnp.float32)
    hidden = (jax.nn.silu(gate_part) * up_part).astype(jnp.bfloat16)
    hidden_all = hidden.reshape(piece.shape[0], piece.shape[1], hidden.shape[1])
    hidden_flat = hidden_all.reshape(-1, hidden_all.shape[-1])
    term = jnp.dot(hidden_flat, down_weight[0], preferred_element_type=jnp.float32)
    summed = lax.psum_scatter(
        term.astype(jnp.bfloat16).astype(jnp.float32).astype(jnp.bfloat16),
        "tp",
        scatter_dimension=0,
        tiled=True,
    )
    expert_out = summed.reshape(sp_count, capacity, width)
    returned_rows = lax.all_to_all(expert_out, "sp", split_axis=0, concat_axis=0, tiled=True)
    weights_own = lax.dynamic_slice_in_dim(route_weights, tp_index * row_count, row_count, 0)
    weight_table = jnp.einsum(
        "rk,rkc->rc", weights_own, table_own.reshape(row_count, TOP_K, sp_count * capacity)
    )
    expert_mix = jnp.dot(
        weight_table,
        returned_rows.reshape(-1, width).astype(jnp.float32),
        precision=lax.Precision.HIGHEST,
    )
    out_own = (after_own.astype(jnp.float32) + expert_mix).astype(jnp.bfloat16)
    return lax.all_gather(out_own, "tp", axis=0, tiled=True)


def solution(mesh):
    placed = (
        P("sp", None),
        P(),
        P(None, "tp"),
        P("tp"),
        P(),
        P("sp", None),
        P("sp", None),
        P("sp", None, "tp"),
        P("sp", None, "tp"),
        P("sp", "tp", None),
    )
    return jax.shard_map(
        shards, mesh=mesh, in_specs=placed, out_specs=P("sp", None), check_vma=False
    )
```

profile of v0, /device:TPU:0, one launch (start us, length us, event | category | flops | bytes accessed | tf_op | source)
XLA Modules:
  0.0 247.7 jit_solution(884471469957618278)
XLA Ops:
  6.5 0.0 copy-start
  6.5 1.6 convert_element_type.65
  8.1 0.0 copy-done.1
  8.2 0.3 multiply_reduce_fusion
  8.5 0.8 dynamic_slice.17
  9.2 0.1 multiply_convert_fusion.1
  9.4 2.4 collective-permute-start
  11.8 0.0 copy-done.3
  11.8 0.1 constant_dynamic-slice_fusion
  11.9 0.1 copy.19
  12.0 0.1 eq.35
  12.1 0.1 fusion.38
  12.2 0.2 reduce_window_sum.11
  12.4 0.2 select_reduce_fusion
  12.6 0.0 collective-permute-done
  12.7 0.1 maximum_convert_fusion
  12.7 0.0 copy-done
  12.7 2.0 fusion.8
  14.7 4.7 %all-to-all-start = ((bf16[4,64,512]{2,1,0:T(8,128)(2,1)}), bf16[4,64,512]{2,1,0:T(8,128)(2,1)S(1)}, u32[]{:S(2)}, u32[]{:S(2)}) async-start(bf16[4,64,512]{2,1,0:T(8,128)(2,1)} %bitcast), calls=%async_computation | async-start | bytes 524288 | tf_op jit(solution)/shard_map/all_to_all | solution.py:76
  19.4 6.0 %all-to-all-done = bf16[4,64,512]{2,1,0:T(8,128)(2,1)S(1)} async-done(((bf16[4,64,512]{2,1,0:T(8,128)(2,1)}), bf16[4,64,512]{2,1,0:T(8,128)(2,1)S(1)}, u32[]{:S(2)}, u32[]{:S(2)}) %all-to-all-start) | async-done | bytes 262176 | tf_op jit(solution)/shard_map/all_to_all | solution.py:76
  25.5 0.2 fusion.9
  25.7 0.1 fusion.11
  25.8 0.3 broadcast_in_dim.32
  26.1 0.2 reshape.66
  26.3 0.5 convolution_convert_fusion.1
  26.9 33.2 %all_to_all.23 = bf16[8,32,2048]{2,1,0:T(8,128)(2,1)} all-to-all(bf16[8,32,2048]{2,1,0:T(8,128)(2,1)S(1)} %bitcast.33), channel_id=1, replica_groups=mesh['sp'=8,'tp'=4] {'sp'}, dimensions={0} | all-to-all | bytes 2097152 | tf_op jit(solution)/shard_map/all_to_all | solution.py:89
  60.0 0.0 all-gather.3.cloned.1.call-update
  60.1 0.0 reduce-scatter.2.cloned.1.call-start
  60.1 50.4 %all-gather.3.cloned.1.call-done = bf16[32,32,2048]{2,1,0:T(8,128)(2,1)} async-done(((bf16[8,32,2048]{2,1,0:T(8,128)(2,1)}), bf16[32,32,2048]{2,1,0:T(8,128)(2,1)}) %all-gather.3.cloned.1.call-update) | async-done | bytes 4194320 | tf_op jit(solution)/shard_map/all_gather | solution.py:90
  110.6 7.5 %fusion.1 = f32[1024,896]{1,0:T(8,128)S(1)} fusion(bf16[1024,2048]{1,0:T(8,128)(2,1)} %bitcast.36, bf16[1,2048,896]{2,1,0:T(8,128)(2,1)} %param.18), kind=kOutput, calls=%fused_computation.2 | convolution fusion | flops 3758096384 | bytes 11534336 | tf_op jit(solution)/shard_map/dot_general | solution.py:93
  118.1 0.0 copy-done.4
  118.1 0.0 copy-done.5
  118.1 0.0 copy-start.6
  118.1 4.7 %multiply_convert_fusion = bf16[1024,896]{1,0:T(8,128)(2,1)S(1)} fusion(f32[1024,896]{1,0:T(8,128)S(1)} %fusion.1, bf16[1024,2048]{1,0:T(8,128)(2,1)S(1)} %bitcast.37, bf16[1,2048,896]{2,1,0:T(8,128)(2,1)S(1)} %copy-done.5), kind=kOutput, calls=%fused_computation.6 | convolution fusion | flops 3763601408 | bytes 13369344 | tf_op jit(solution)/shard_map/dot_general | solution.py:92
  122.9 6.0 %convolution_convert_fusion = bf16[1024,2048]{1,0:T(8,128)(2,1)} fusion(bf16[1024,896]{1,0:T(8,128)(2,1)S(1)} %multiply_convert_fusion, bf16[1,896,2048]{2,1,0:T(8,128)(2,1)S(1)} %copy-done.6), kind=kOutput, calls=%fused_computation | convolution fusion | flops 3760193536 | bytes 9699328 | tf_op jit(solution)/shard_map/dot_general | solution.py:97
  128.9 0.0 reduce-scatter.2.cloned.1.call-update
  128.9 52.8 %reduce-scatter.2.cloned.1.call-done = bf16[256,2048]{1,0:T(8,128)(2,1)} async-done(((bf16[1024,2048]{1,0:T(8,128)(2,1)}), bf16[256,2048]{1,0:T(8,128)(2,1)}) %reduce-scatter.2.cloned.1.call-update) | async-done | bytes 1048592 | tf_op jit(solution)/shard_map/reduce_scatter | solution.py:98
  181.7 4.6 %all-to-all-start.2 = ((bf16[8,32,2048]{2,1,0:T(8,128)(2,1)}), bf16[8,32,2048]{2,1,0:T(8,128)(2,1)S(1)}, u32[]{:S(2)}, u32[]{:S(2)}) async-start(bf16[8,32,2048]{2,1,0:T(8,128)(2,1)} %bitcast.35), calls=%async_computation.3 | async-start | bytes 2097152 | tf_op jit(solution)/shard_map/all_to_all | solution.py:105
  186.3 0.0 all-gather.5.cloned.1.call-start
  186.3 0.1 reduce_sum.31
  186.5 0.8 dynamic-slice_bitcast_fusion
  187.2 0.1 copy.17
  187.4 0.3 fusion.30
  187.7 25.2 %all-to-all-done.2 = bf16[8,32,2048]{2,1,0:T(8,128)(2,1)S(1)} async-done(((bf16[8,32,2048]{2,1,0:T(8,128)(2,1)}), bf16[8,32,2048]{2,1,0:T(8,128)(2,1)S(1)}, u32[]{:S(2)}, u32[]{:S(2)}) %all-to-all-start.2) | async-done | bytes 1048608 | tf_op jit(solution)/shard_map/all_to_all | solution.py:105
  212.9 1.4 fusion.7
  214.2 0.0 all-gather.5.cloned.1.call-update
  214.3 24.6 %all-gather.5.cloned.1.call-done = bf16[256,2048]{1,0:T(8,128)(2,1)} async-done(((bf16[64,2048]{1,0:T(8,128)(2,1)}), bf16[256,2048]{1,0:T(8,128)(2,1)}) %all-gather.5.cloned.1.call-update) | async-done | bytes 1048592 | tf_op jit(solution)/shard_map/all_gather | solution.py:116
  238.9 2.3 copy.26
  (18 shorter events, 0.1 us)
Async XLA Ops:
  6.5 6.2 %copy-start = (bf16[512,512]{1,0:T(8,128)(2,1)S(1)}, bf16[512,512]{1,0:T(8,128)(2,1)}, u32[]{:S(2)}) copy-start(bf16[512,512]{1,0:T(8,128)(2,1)} %param.12) | copy-start | bytes 1572868
  6.5 5.3 %copy-start.3 = (s32[256,2]{0,1:T(2,128)S(1)}, s32[256,2]{0,1:T(2,128)}, u32[]{:S(2)}) copy-start(s32[256,2]{0,1:T(2,128)} %param.15) | copy-start | bytes 6148
  6.5 6.2 %copy-start.7 = (f32[512]{0:T(512)S(1)}, f32[512]{0:T(512)}, u32[]{:S(2)}) copy-start(f32[512]{0:T(512)} %param.13) | copy-start | bytes 6148
  6.5 1.6 copy-start.1
  9.4 3.3 %collective-permute-start = (bf16[16,512]{1,0:T(8,128)(2,1)S(1)}, bf16[16,512]{1,0:T(8,128)(2,1)S(1)}, u32[]{:S(2)}, u32[]{:S(2)}) collective-permute-start(bf16[16,512]{1,0:T(8,128)(2,1)S(1)} %slice.69), channel_id=1, source_target_pairs={{0,4},{4,8},{8,12},{12,16},{16,20},{20,24},{24,28},{1,5},{5,9},{9,... | collective-permute-start | bytes 49160 | tf_op jit(solution)/shard_map/ppermute | solution.py:17
  14.7 10.9 %copy-start.2 = (f32[2048]{0:T(1024)S(1)}, f32[2048]{0:T(1024)}, u32[]{:S(2)}) copy-start(f32[2048]{0:T(1024)} %param.14) | copy-start | bytes 24580
  14.7 10.6 %all-to-all-start = ((bf16[4,64,512]{2,1,0:T(8,128)(2,1)}), bf16[4,64,512]{2,1,0:T(8,128)(2,1)S(1)}, u32[]{:S(2)}, u32[]{:S(2)}) async-start(bf16[4,64,512]{2,1,0:T(8,128)(2,1)} %bitcast), calls=%async_computation | async-start | bytes 524288 | tf_op jit(solution)/shard_map/all_to_all | solution.py:76
  19.4 91.1 %all-gather.3.cloned.1.call-start = ((), (), s32[]{:S(2)}) async-start(), calls=%async_computation.4 | async-start | bytes 5242880 | tf_op jit(solution)/shard_map/all_gather | solution.py:90
  60.1 121.6 %reduce-scatter.2.cloned.1.call-start = ((), (), s32[]{:S(2)}) async-start(), calls=%async_computation.5 | async-start | bytes 5242880 | tf_op jit(solution)/shard_map/reduce_scatter | solution.py:98
  110.6 7.5 %copy-start.4 = (bf16[32,32,2048]{2,1,0:T(8,128)(2,1)S(1)}, bf16[32,32,2048]{2,1,0:T(8,128)(2,1)}, u32[]{:S(2)}) copy-start(bf16[32,32,2048]{2,1,0:T(8,128)(2,1)} %all-gather.3.cloned.1.call-done) | copy-start | bytes 12582916
  110.6 7.5 %copy-start.5 = (bf16[1,2048,896]{2,1,0:T(8,128)(2,1)S(1)}, bf16[1,2048,896]{2,1,0:T(8,128)(2,1)}, u32[]{:S(2)}) copy-start(bf16[1,2048,896]{2,1,0:T(8,128)(2,1)} %param.17) | copy-start | bytes 11010052
  118.1 4.8 %copy-start.6 = (bf16[1,896,2048]{2,1,0:T(8,128)(2,1)S(1)}, bf16[1,896,2048]{2,1,0:T(8,128)(2,1)}, u32[]{:S(2)}) copy-start(bf16[1,896,2048]{2,1,0:T(8,128)(2,1)} %param.19) | copy-start | bytes 11010052
  181.7 31.2 %all-to-all-start.2 = ((bf16[8,32,2048]{2,1,0:T(8,128)(2,1)}), bf16[8,32,2048]{2,1,0:T(8,128)(2,1)S(1)}, u32[]{:S(2)}, u32[]{:S(2)}) async-start(bf16[8,32,2048]{2,1,0:T(8,128)(2,1)} %bitcast.35), calls=%async_computation.3 | async-start | bytes 2097152 | tf_op jit(solution)/shard_map/all_to_all | solution.py:105
  186.3 52.6 %all-gather.5.cloned.1.call-start = ((), (), s32[]{:S(2)}) async-start(), calls=%async_computation.6 | async-start | bytes 1310720 | tf_op jit(solution)/shard_map/all_gather | solution.py:116
Sparse Core Ops, SparseCore 0:
  60.2 50.3 all-gather.2
  129.1 52.5 reduce-scatter.1
  214.4 24.4 all-gather.4
where the time goes:
time: 248 us
  waiting for transfers between devices  159 us (64%)
  blocking collectives  33.2 us (13%)
  matrix products  22.5 us (9%)
  between operations  13.4 us (5%)
  starting transfers between devices  11.8 us (5%)
  local copies, waits for them, and re-layouts  5 us (2%)
  other arithmetic  2.84 us (1%)
    reduce_scatter x1, waiting for transfers between devices, shards(): lax.psum_scatter(term.astype(jnp.bfloat16).astype(jnp.float32).astype(jnp...  52.8 us
    all_gather x1, waiting for transfers between devices, shards(): piece = lax.all_gather(arrived, 'tp', axis=0, tiled=True)  50.4 us
    all_to_all x1, blocking collectives, shards(): lax.all_to_all(outgoing, 'sp', split_axis=0, concat_axis=0, tiled=True)  33.2 us
    all_to_all x1, waiting for transfers between devices, shards(): lax.all_to_all(expert_out, 'sp', split_axis=0, concat_axis=0, tiled=True)  25.2 us
    all_gather x1, waiting for transfers between devices, shards(): return lax.all_gather(out_own, 'tp', axis=0, tiled=True)  24.6 us
    dot_general x1, matrix products, shards(): jnp.dot(flat_rows, up_weight[0], preferred_element_type=jnp.float32)  7.49 us
    dot_general x1, matrix products, shards(): jnp.dot(hidden_flat, down_weight[0], preferred_element_type=jnp.float32)  6.05 us
    all_to_all x1, waiting for transfers between devices, shards(): lax.all_to_all(mixed, 'tp', split_axis=0, concat_axis=1, tiled=True)  5.96 us
  transfers between devices with their start and end apart: 6, of which 5 were waited for; matrix products, arithmetic and copies ran while one was open for 1% of the time, Pallas kernels for 0%

commit v1 on v0

--- a/solution.py
+++ b/solution.py
@@ -1,15 +1,20 @@
+import functools
+
 import jax
 import jax.numpy as jnp
 from jax import lax
+from jax.experimental import pallas as pl
+from jax.experimental.pallas import tpu as pltpu
 from jax.sharding import PartitionSpec as P
 
 GROUPS = 4
 SPAN = 16
 TOP_K = 2
-
-
+CORES = 2
+SIDE = 2
 EPS = 1e-06
-
+MESH = pl.DeviceIdType.MESH
+ZU, ZD, X, Y, DX, DY, FX, FY, FDX, FDY = range(10)
 
 def from_behind(value, axis, steps):
     count = lax.axis_size(axis)
@@ -32,7 +37,7 @@
     )
 
 
-def shards(
+def shards_any(
     residual_in,
     mix_gain,
     pool_weight,
@@ -116,6 +121,493 @@
     return lax.all_gather(out_own, "tp", axis=0, tiled=True)
 
 
+class Place:
+    def __init__(self, send_sem, recv_sem):
+        self.sp, self.tp = lax.axis_index("sp"), lax.axis_index("tp")
+        self.levels = lax.axis_size("sp") // CORES
+        self.z, self.c = self.sp // CORES, self.sp % CORES
+        y, x = self.tp // SIDE, self.tp % SIDE
+        self.tx = y * SIDE + (1 - x)
+        self.ty = (1 - y) * SIDE + x
+        self.td = (1 - y) * SIDE + (1 - x)
+        self.send_sem, self.recv_sem = send_sem, recv_sem
+        partner = self.z * CORES + (1 - self.c)
+        self.partner = (partner, self.tp)
+        self.to = {
+            ZU: (self.sp + CORES, self.tp),
+            ZD: (self.sp - CORES, self.tp),
+            X: (self.sp, self.tx),
+            Y: (self.sp, self.ty),
+        }
+        for kind, base in ((DX, X), (DY, Y), (FX, X), (FY, Y), (FDX, X), (FDY, Y)):
+            self.to[kind] = self.to[base]
+
+    def copy(self, kind, index, src, dst):
+        return pltpu.make_async_remote_copy(
+            src_ref=src,
+            dst_ref=dst,
+            send_sem=self.send_sem.at[kind, index],
+            recv_sem=self.recv_sem.at[kind, index],
+            device_id=self.to[kind],
+            device_id_type=MESH,
+        )
+
+    def exists(self, offset):
+        level = self.z + offset
+        return (level >= 0) & (level < self.levels)
+
+    def offsets(self):
+        order = [0]
+        for distance in range(1, self.levels):
+            order += [-distance, distance]
+        return order
+
+
+def greet(place, everyone):
+    barrier = pltpu.get_barrier_semaphore()
+
+    def hello(target):
+        pl.semaphore_signal(barrier, inc=1, device_id=target, device_id_type=MESH)
+
+    hello(place.to[X])
+    hello(place.to[Y])
+    if everyone:
+        count = lax.axis_size("sp")
+        for step in range(1, count):
+            hello((lax.rem(place.sp + step, count), place.tp))
+        pl.semaphore_wait(barrier, count + 1)
+    else:
+        hello(place.partner)
+        up, down = place.exists(1), place.exists(-1)
+        pl.when(up)(lambda: hello(place.to[ZU]))
+        pl.when(down)(lambda: hello(place.to[ZD]))
+        pl.semaphore_wait(barrier, 3 + up.astype(jnp.int32) + down.astype(jnp.int32))
+
+
+def gather_kernel(
+    own_ref, meta_ref, out_ref, meta_out, send_sem, recv_sem, p_send, p_recv, m_send, m_recv, l_sem
+):
+    place = Place(send_sem, recv_sem)
+    rows, cols = own_ref.shape
+    half = rows // 2
+    z, c, tp = place.z, place.c, place.tp
+    sp_count = lax.axis_size("sp")
+    tiles = SIDE * SIDE
+
+    def block(level, core, tile, first=0, count=rows):
+        start = pl.multiple_of((level * CORES + core) * rows + first, half)
+        return out_ref.at[pl.ds(start, count), pl.ds(pl.multiple_of(tile * cols, cols), cols)]
+
+    def pair_copy(level, tile, core):
+        ref = block(level, core, tile)
+        return pltpu.make_async_remote_copy(
+            src_ref=ref,
+            dst_ref=ref,
+            send_sem=p_send.at[level, tile],
+            recv_sem=p_recv.at[level, tile],
+            device_id=place.partner,
+            device_id_type=MESH,
+        )
+
+    def meta_copy(step):
+        target = lax.rem(place.sp + step, sp_count)
+        return pltpu.make_async_remote_copy(
+            src_ref=meta_ref,
+            dst_ref=meta_out.at[place.sp],
+            send_sem=m_send.at[step],
+            recv_sem=m_recv.at[step],
+            device_id=(target, tp),
+            device_id_type=MESH,
+        )
+
+    local = pltpu.make_async_copy(own_ref, block(z, c, tp), l_sem.at[0])
+    local.start()
+    local_meta = pltpu.make_async_copy(meta_ref, meta_out.at[place.sp], l_sem.at[1])
+    local_meta.start()
+    local.wait()
+    local_meta.wait()
+    greet(place, True)
+
+    def whole(kind, level, tile):
+        ref = block(level, c, tile)
+        return place.copy(kind, level, ref, ref)
+
+    def part(kind, level, tile):
+        ref = block(level, c, tile, 0 if kind == DY else half, half)
+        return place.copy(kind, level, ref, ref)
+
+    def first(offset):
+        level = z + offset
+        if offset < 0:
+            whole(ZU, level, tp).wait_recv()
+        if offset > 0:
+            whole(ZD, level, tp).wait_recv()
+        if offset <= 0:
+            pl.when(place.exists(1))(lambda: whole(ZU, level, tp).start())
+        if offset >= 0:
+            pl.when(place.exists(-1))(lambda: whole(ZD, level, tp).start())
+        whole(X, level, tp).start()
+        whole(Y, level, tp).start()
+        pair_copy(level, tp, c).start()
+
+    def second(offset):
+        level = z + offset
+        whole(X, level, place.tx).wait_recv()
+        part(DY, level, place.tx).start()
+        pair_copy(level, place.tx, c).start()
+        whole(Y, level, place.ty).wait_recv()
+        part(DX, level, place.ty).start()
+        pair_copy(level, place.ty, c).start()
+
+    def third(offset):
+        level = z + offset
+        part(DY, level, place.td).wait_recv()
+        part(DX, level, place.td).wait_recv()
+        pair_copy(level, place.td, c).start()
+
+    order = place.offsets()
+    for step in range(len(order) + 2):
+        if step < len(order):
+            pl.when(place.exists(order[step]))(functools.partial(first, order[step]))
+        if step == 0:
+            for hop in range(1, sp_count):
+                meta_copy(hop).start()
+        if 0 <= step - 1 < len(order):
+            pl.when(place.exists(order[step - 1]))(functools.partial(second, order[step - 1]))
+        if 0 <= step - 2 < len(order):
+            pl.when(place.exists(order[step - 2]))(functools.partial(third, order[step - 2]))
+
+    for hop in range(1, sp_count):
+        meta_copy(hop).wait_send()
+        meta_copy(hop).wait_recv()
+
+    def sent(offset):
+        level = z + offset
+        if offset <= 0:
+            pl.when(place.exists(1))(lambda: whole(ZU, level, tp).wait_send())
+        if offset >= 0:
+            pl.when(place.exists(-1))(lambda: whole(ZD, level, tp).wait_send())
+        whole(X, level, tp).wait_send()
+        whole(Y, level, tp).wait_send()
+        part(DY, level, place.tx).wait_send()
+        part(DX, level, place.ty).wait_send()
+
+    for offset in order:
+        pl.when(place.exists(offset))(functools.partial(sent, offset))
+    for level in range(place.levels):
+        for tile in range(tiles):
+            pair_copy(level, tile, c).wait_send()
+            pair_copy(level, tile, 1 - c).wait_recv()
+
+
+def gather_all(own, meta, sp_count, tp_count):
+    rows, cols = own.shape
+    levels = sp_count // CORES
+    vmem = pl.BlockSpec(memory_space=pltpu.VMEM)
+    return pl.pallas_call(
+        gather_kernel,
+        out_shape=(
+            jax.ShapeDtypeStruct((sp_count * rows, tp_count * cols), own.dtype),
+            jax.ShapeDtypeStruct((sp_count,) + meta.shape, meta.dtype),
+        ),
+        in_specs=[vmem, vmem],
+        out_specs=(vmem, vmem),
+        scratch_shapes=[
+            pltpu.SemaphoreType.DMA((6, levels)),
+            pltpu.SemaphoreType.DMA((6, levels)),
+            pltpu.SemaphoreType.DMA((levels, tp_count)),
+            pltpu.SemaphoreType.DMA((levels, tp_count)),
+            pltpu.SemaphoreType.DMA((sp_count,)),
+            pltpu.SemaphoreType.DMA((sp_count,)),
+            pltpu.SemaphoreType.DMA((2,)),
+        ],
+        compiler_params=pltpu.CompilerParams(collective_id=0, has_side_effects=True),
+        name="gather_all",
+    )(own, meta)
+
+
+def combine_kernel(
+    part_ref, after_ref, out_ref,
+    r_pair, s_diag, r_ydiag, r_xdiag, s_x, s_y, r_x, r_y, s_z, r_up, r_down,
+    send_sem, recv_sem, p_send, p_recv,
+):
+    place = Place(send_sem, recv_sem)
+    rows, cols = after_ref.shape
+    half = rows // 2
+    z, c, tp = place.z, place.c, place.tp
+    chunk = 32
+
+    pl.when(z == 0)(lambda: r_up.__setitem__(Ellipsis, jnp.zeros_like(r_up)))
+    pl.when(z == place.levels - 1)(lambda: r_down.__setitem__(Ellipsis, jnp.zeros_like(r_down)))
+    greet(place, False)
+
+    def pair_copy(level):
+        start = pl.multiple_of((level * CORES + (1 - c)) * rows, rows)
+        return pltpu.make_async_remote_copy(
+            src_ref=part_ref.at[pl.ds(start, rows)],
+            dst_ref=r_pair.at[level],
+            send_sem=p_send.at[level],
+            recv_sem=p_recv.at[level],
+            device_id=place.partner,
+            device_id_type=MESH,
+        )
+
+    def summed(level, tile, row, count=chunk):
+        start = pl.multiple_of((level * CORES + c) * rows + row, chunk)
+        lanes = pl.ds(pl.multiple_of(tile * cols, cols), cols)
+        mine = part_ref[pl.ds(start, count), lanes].astype(jnp.float32)
+        return mine + r_pair[level, pl.ds(pl.multiple_of(row, chunk), count), lanes].astype(
+            jnp.float32
+        )
+
+    def over(first, last, body):
+        def step(index, carry):
+            body(pl.multiple_of(first + index * chunk, chunk))
+            return carry
+
+        lax.fori_loop(0, (last - first) // chunk, step, 0)
+
+    def diag(kind, level):
+        if kind == DY:
+            return place.copy(kind, level, s_diag.at[level, pl.ds(0, half)], r_ydiag.at[level])
+        return place.copy(kind, level, s_diag.at[level, pl.ds(half, half)], r_xdiag.at[level])
+
+    def side(kind, level):
+        if kind == X:
+            return place.copy(kind, level, s_x.at[level], r_x.at[level])
+        return place.copy(kind, level, s_y.at[level], r_y.at[level])
+
+    def line(kind, level):
+        return place.copy(kind, level, s_z.at[level], (r_up if kind == ZU else r_down).at[level])
+
+    def first(offset):
+        level = z + offset
+        pair_copy(level).wait_recv()
+
+        def body(row):
+            s_diag[level, pl.ds(row, chunk)] = summed(level, place.td, row).astype(jnp.bfloat16)
+
+        over(0, half, body)
+        diag(DY, level).start()
+        over(half, rows, body)
+        diag(DX, level).start()
+
+    def second(offset):
+        level = z + offset
+
+        def plain(buffer, tile):
+            def body(row):
+                buffer[level, pl.ds(row, chunk)] = summed(level, tile, row).astype(jnp.bfloat16)
+
+            return body
+
+        def joined(buffer, tile, arrived, base):
+            def body(row):
+                other = arrived[level, pl.ds(pl.multiple_of(row - base, chunk), chunk)]
+                total = summed(level, tile, row) + other.astype(jnp.float32)
+                buffer[level, pl.ds(row, chunk)] = total.astype(jnp.bfloat16)
+
+            return body
+
+        over(half, rows, plain(s_x, place.tx))
+        over(0, half, plain(s_y, place.ty))
+        diag(DY, level).wait_recv()
+        over(0, half, joined(s_x, place.tx, r_ydiag, 0))
+        side(X, level).start()
+        diag(DX, level).wait_recv()
+        over(half, rows, joined(s_y, place.ty, r_xdiag, half))
+        side(Y, level).start()
+
+    def third(offset):
+        level = z + offset
+        side(X, level).wait_recv()
+        side(Y, level).wait_recv()
+        if offset >= 0:
+            pl.when(z > 0)(lambda: line(ZU, level).wait_recv())
+        if offset <= 0:
+            pl.when(z < place.levels - 1)(lambda: line(ZD, level).wait_recv())
+
+        def body(row):
+            at = pl.ds(row, chunk)
+            total = summed(level, tp, row)
+            total = total + r_x[level, at].astype(jnp.float32) + r_y[level, at].astype(jnp.float32)
+            if offset >= 0:
+                total = total + r_up[level, at].astype(jnp.float32)
+            if offset <= 0:
+                total = total + r_down[level, at].astype(jnp.float32)
+            if offset == 0:
+                total = total + after_ref[at].astype(jnp.float32)
+                lanes = pl.ds(pl.multiple_of(tp * cols, cols), cols)
+                out_ref[at, lanes] = total.astype(jnp.bfloat16)
+            else:
+                s_z[level, at] = total.astype(jnp.bfloat16)
+
+        over(0, rows, body)
+        if offset > 0:
+            line(ZU, level).start()
+        if offset < 0:
+            line(ZD, level).start()
+
+    order = place.offsets()[::-1]
+    for offset in order:
+        pl.when(place.exists(offset))(lambda offset=offset: pair_copy(z + offset).start())
+    for step in range(len(order) + 2):
+        if step < len(order):
+            pl.when(place.exists(order[step]))(functools.partial(first, order[step]))
+        if 0 <= step - 1 < len(order):
+            pl.when(place.exists(order[step - 1]))(functools.partial(second, order[step - 1]))
+        if 0 <= step - 2 < len(order):
+            pl.when(place.exists(order[step - 2]))(functools.partial(third, order[step - 2]))
+
+    def final(kind, tile):
+        start, count = {FX: (0, rows), FY: (0, rows), FDY: (0, half), FDX: (half, half)}[kind]
+        ref = out_ref.at[pl.ds(start, count), pl.ds(pl.multiple_of(tile * cols, cols), cols)]
+        return place.copy(kind, 0, ref, ref)
+
+    final(FX, tp).start()
+    final(FY, tp).start()
+
+    def sent(offset):
+        level = z + offset
+        pair_copy(level).wait_send()
+        for kind in (DX, DY):
+            diag(kind, level).wait_send()
+        for kind in (X, Y):
+            side(kind, level).wait_send()
+        if offset > 0:
+            line(ZU, level).wait_send()
+        if offset < 0:
+            line(ZD, level).wait_send()
+
+    final(FX, place.tx).wait_recv()
+    final(FDY, place.tx).start()
+    final(FY, place.ty).wait_recv()
+    final(FDX, place.ty).start()
+    for offset in order:
+        pl.when(place.exists(offset))(functools.partial(sent, offset))
+    final(FDY, place.td).wait_recv()
+    final(FDX, place.td).wait_recv()
+    final(FX, tp).wait_send()
+    final(FY, tp).wait_send()
+    final(FDY, place.tx).wait_send()
+    final(FDX, place.ty).wait_send()
+
+
+def combine_all(parts, after, sp_count, tp_count):
+    rows, cols = after.shape
+    levels = sp_count // CORES
+    vmem = pl.BlockSpec(memory_space=pltpu.VMEM)
+    whole = pltpu.VMEM((levels, rows, cols), jnp.bfloat16)
+    halved = pltpu.VMEM((levels, rows // 2, cols), jnp.bfloat16)
+    return pl.pallas_call(
+        combine_kernel,
+        out_shape=jax.ShapeDtypeStruct((rows, tp_count * cols), after.dtype),
+        in_specs=[vmem, vmem],
+        out_specs=vmem,
+        scratch_shapes=[
+            pltpu.VMEM((levels, rows, tp_count * cols), jnp.bfloat16),
+            whole, halved, halved, whole, whole, whole, whole, whole, whole, whole,
+            pltpu.SemaphoreType.DMA((10, levels)),
+            pltpu.SemaphoreType.DMA((10, levels)),
+            pltpu.SemaphoreType.DMA((levels,)),
+            pltpu.SemaphoreType.DMA((levels,)),
+        ],
+        compiler_params=pltpu.CompilerParams(collective_id=1, has_side_effects=True),
+        name="combine_all",
+    )(parts, after)
+
+
+def shards(
+    residual_in,
+    mix_gain,
+    pool_weight,
+    pool_scale,
+    ffn_gain,
+    route_ids,
+    route_weights,
+    gate_weight,
+    up_weight,
+    down_weight,
+):
+    tp_count = lax.axis_size("tp")
+    sp_count = lax.axis_size("sp")
+    tp_index = lax.axis_index("tp")
+    tok_count, width = residual_in.shape
+    group_width = width // GROUPS
+    col_count = pool_weight.shape[1]
+    block_rows = tok_count // tp_count
+    capacity = 2 * TOP_K * block_rows // sp_count
+    group_index = tp_index * col_count // group_width
+    window = jnp.power(2, group_index + 1)
+    stream = residual_in.astype(jnp.float32)
+    inverse = lax.rsqrt(jnp.mean(stream * stream, axis=-1, keepdims=True) + EPS)
+    stream_group = lax.dynamic_slice_in_dim(stream, group_index * group_width, group_width, 1)
+    gain_group = lax.dynamic_slice_in_dim(mix_gain, group_index * group_width, group_width, 0)
+    normed_group = (stream_group * inverse * gain_group).astype(jnp.bfloat16)
+    rim_rows = from_behind(normed_group[tok_count - SPAN :], "sp", 1)
+    extended = jnp.concatenate([rim_rows, normed_group], axis=0).astype(jnp.float32)
+    window_sum = jnp.zeros((tok_count, group_width), jnp.float32)
+    for offset in range(SPAN):
+        window_sum = window_sum + jnp.where(
+            offset < window, extended[SPAN - offset : SPAN - offset + tok_count], 0.0
+        )
+    position = lax.axis_index("sp") * tok_count + jnp.arange(tok_count, dtype=jnp.int32)
+    divisor = jnp.minimum(position + 1, window).astype(jnp.float32)
+    pooled = (window_sum / divisor[:, None] - extended[SPAN:]).astype(jnp.bfloat16)
+    mixed = (jnp.dot(pooled, pool_weight, preferred_element_type=jnp.float32) * pool_scale).astype(
+        jnp.bfloat16
+    )
+    stream_own = lax.dynamic_slice_in_dim(stream, tp_index * col_count, col_count, 1)
+    after_own = (stream_own + mixed.astype(jnp.float32)).astype(jnp.bfloat16)
+
+    meta = jnp.concatenate(
+        [
+            route_ids.astype(jnp.float32).T,
+            route_weights.T,
+            jnp.zeros((8 - 2 * TOP_K, tok_count), jnp.float32),
+        ],
+        axis=0,
+    )
+    after_all, meta_all = gather_all(after_own, meta, sp_count, tp_count)
+
+    expert = lax.axis_index("sp").astype(jnp.float32)
+    named = (meta_all[:, :TOP_K] == expert).astype(jnp.float32)
+    match = jnp.sum(named, axis=1)
+    weight = jnp.sum(named * meta_all[:, TOP_K : 2 * TOP_K], axis=1)
+    at = jnp.arange(tok_count, dtype=jnp.int32)
+    earlier = (at[:, None] < at[None, :]) & (at[:, None] // block_rows == at[None, :] // block_rows)
+    before = jnp.dot(
+        match.astype(jnp.bfloat16),
+        earlier.astype(jnp.bfloat16),
+        preferred_element_type=jnp.float32,
+    )
+    slots = capacity * tp_count
+    slot_of = before + (at // block_rows * capacity).astype(jnp.float32)[None, :]
+    slot_of = jnp.where(match > 0, slot_of, -1.0)
+    chosen = slot_of[:, None, :] == jnp.arange(slots, dtype=jnp.float32)[None, :, None]
+    table = chosen.astype(jnp.bfloat16)
+    slot_weight = jnp.sum(jnp.where(chosen, weight[:, None, :], 0.0), axis=-1).reshape(-1, 1)
+    picked = lax.dot_general(
+        table,
+        after_all.reshape(sp_count, tok_count, width),
+        (((2,), (1,)), ((0,), (0,))),
+        preferred_element_type=jnp.float32,
+    ).reshape(-1, width)
+    flat_rows = rms_scale(picked, ffn_gain).astype(jnp.bfloat16)
+    gate_part = jnp.dot(flat_rows, gate_weight[0], preferred_element_type=jnp.float32)
+    up_part = jnp.dot(flat_rows, up_weight[0], preferred_element_type=jnp.float32)
+    hidden = (jax.nn.silu(gate_part) * up_part).astype(jnp.bfloat16)
+    term = jnp.dot(hidden, down_weight[0], preferred_element_type=jnp.float32)
+    term = (term * slot_weight).astype(jnp.bfloat16)
+    parts = lax.dot_general(
+        table,
+        term.reshape(sp_count, slots, width),
+        (((1,), (1,)), ((0,), (0,))),
+        preferred_element_type=jnp.float32,
+    ).astype(jnp.bfloat16)
+    return combine_all(parts.reshape(-1, width), after_own, sp_count, tp_count)
+
+
 def solution(mesh):
     placed = (
         P("sp", None),
@@ -129,6 +621,11 @@
         P("sp", None, "tp"),
         P("sp", "tp", None),
     )
+    square = mesh.shape["tp"] == SIDE * SIDE and mesh.shape["sp"] % CORES == 0
     return jax.shard_map(
-        shards, mesh=mesh, in_specs=placed, out_specs=P("sp", None), check_vma=False
-    )
+        shards if square else shards_any,
+        mesh=mesh,
+        in_specs=placed,
+        out_specs=P("sp", None),
+        check_vma=False,
+    )

time: 248 us -> 161 us (0.65)
  waiting for transfers between devices: 159 us -> 0.01 us
  Pallas kernels: 0 us -> 120 us
  blocking collectives: 33.2 us -> 0 us
  between operations: 13.4 us -> 0.3 us
  starting transfers between devices: 11.8 us -> 2.4 us
  matrix products: 22.5 us -> 26.4 us
  other arithmetic: 2.84 us -> 6.25 us
    pallas_call x0 -> x2, Pallas kernels: none -> 120 us  [the longest x1 63.2 us: combine_all(): pl.pallas_call(combine_kernel, out_shape=jax.ShapeDtypeStruct((rows, tp_c...]
    all_gather x2 -> x0, waiting for transfers between devices: 75.1 us -> none  [the longest x1 50.4 us: shards(): piece = lax.all_gather(arrived, 'tp', axis=0, tiled=True)]
    reduce_scatter x1 -> x0, waiting for transfers between devices: 52.8 us -> none  [shards(): lax.psum_scatter(term.astype(jnp.bfloat16).astype(jnp.float32).astype(jnp...]
    all_to_all x1 -> x0, blocking collectives: 33.2 us -> none  [shards(): lax.all_to_all(outgoing, 'sp', split_axis=0, concat_axis=0, tiled=True)]
    all_to_all x2 -> x0, waiting for transfers between devices: 31.1 us -> none  [the longest x1 25.2 us: shards(): lax.all_to_all(expert_out, 'sp', split_axis=0, concat_axis=0, tiled=True)]
    all_to_all x2 -> x0, starting transfers between devices: 9.27 us -> none  [the longest x1 4.67 us: shards(): lax.all_to_all(mixed, 'tp', split_axis=0, concat_axis=1, tiled=True)]
    dot_general x4, matrix products: 8.23 us -> 15.2 us  [the longest x1 5.59 us: shards(): lax.dot_general(table, term.reshape(sp_count, slots, width), (((1,), (1,)...]
    dot_general x1, matrix products: 7.49 us -> 4.49 us  [shards(): jnp.dot(flat_rows, up_weight[0], preferred_element_type=jnp.float32)]
  transfers between devices with their start and end apart: 6 -> 1, of which waited for: 5 -> 0; matrix products, arithmetic and copies ran while one was open for 1% -> 0% of each run, Pallas kernels for 0% -> 0%
where the time goes in v1:
time: 161 us; the launch traced here: 160 us
  Pallas kernels  120 us (75%)
  matrix products  26.4 us (16%)
  other arithmetic  6.25 us (4%)
  local copies, waits for them, and re-layouts  4.43 us (3%)
  starting transfers between devices  2.4 us (1%)
    pallas_call x1, Pallas kernels, combine_all(): pl.pallas_call(combine_kernel, out_shape=jax.ShapeDtypeStruct((rows, tp_c...  63.2 us
    pallas_call x1, Pallas kernels, gather_all(): pl.pallas_call(gather_kernel, out_shape=(jax.ShapeDtypeStruct((sp_count *...  57.3 us
    dot_general x1, matrix products, shards(): lax.dot_general(table, term.reshape(sp_count, slots, width), (((1,), (1,)...  5.59 us
    dot_general x1, matrix products, shards(): jnp.dot(flat_rows, gate_weight[0], preferred_element_type=jnp.float32)  4.77 us
    dot_general x1, matrix products, shards(): term = jnp.dot(hidden, down_weight[0], preferred_element_type=jnp.float32)  4.71 us
    dot_general x1, matrix products, shards(): lax.dot_general(table, after_all.reshape(sp_count, tok_count, width), (((...  4.64 us
    dot_general x1, matrix products, shards(): jnp.dot(flat_rows, up_weight[0], preferred_element_type=jnp.float32)  4.49 us
    unnamed x17, local copies, waits for them, and re-layouts  3.58 us
  transfers between devices with their start and end apart: 1, of which 0 were waited for; matrix products, arithmetic and copies ran while one was open for 0% of the time, Pallas kernels for 0%

profile of v1, /device:TPU:0, one launch (start us, length us, event | category | flops | bytes accessed | tf_op | source)
XLA Modules:
  0.0 160.3 jit_solution(3651108397130147293)
XLA Ops:
  0.0 0.0 copy-start
  0.0 0.0 copy-start.3
  0.0 0.0 copy-start.2
  0.0 0.0 copy-start.7
  0.0 1.6 multiply_reduce_fusion.1
  1.6 1.5 convert_element_type.65
  3.1 0.8 dynamic_slice.11
  3.9 0.1 multiply_convert_fusion.3
  4.0 2.4 %collective-permute-start = (bf16[16,512]{1,0:T(8,128)(2,1)S(1)}, bf16[16,512]{1,0:T(8,128)(2,1)S(1)}, u32[]{:S(2)}, u32[]{:S(2)}) collective-permute-start(bf16[16,512]{1,0:T(8,128)(2,1)S(1)} %slice.77), channel_id=1, source_target_pairs={{0,4},{4,8},{8,12},{12,16},{16,20},{20,24},{24,28},{1,5},{5,9},{9,... | collective-permute-start | bytes 49160 | tf_op jit(solution)/shard_map/ppermute | solution.py:22
  6.4 0.0 copy-done.3
  6.5 0.1 pad.2.clone
  6.6 0.0 copy-done.2
  6.6 0.7 maximum_maximum_fusion.meta_ref
  7.2 0.0 collective-permute-done
  7.2 0.1 maximum_convert_fusion
  7.3 0.0 copy-done
  7.3 0.0 copy-done.7
  7.3 2.0 %fusion.10.own_ref.after_ref = bf16[256,512]{1,0:T(8,128)(2,1)} fusion(bf16[512,512]{1,0:T(8,128)(2,1)S(1)} %copy-done, f32[256,2048]{1,0:T(8,128)S(1)} %convert_element_type.65, s32[]{:T(128)S(6)} %select_n.166, f32[512]{0:T(512)S(1)} %copy-done.7, f32[272,512]{1,0:T(8,128)S(1)} %maximum_convert_fusion, f32[256]{0:T(256)S(1)} %minimum_convert_fusion, ...), kind=kOutput, calls=%fused_computation.15 | convolution fusion | flops 139329536 | bytes 9702420 | tf_op jit(solution)/shard_map/dot_general | solution.py:557
  9.3 57.3 %gather_all.1 = (bf16[2048,2048]{1,0:T(8,128)(2,1)}, f32[8,8,256]{2,1,0:T(8,128)}) custom-call(bf16[256,512]{1,0:T(8,128)(2,1)} %fusion.10.own_ref.after_ref, f32[8,256]{1,0:T(8,128)} %maximum_maximum_fusion.meta_ref), custom_call_target="tpu_custom_call" | custom-call | tf_op jit(solution)/shard_map/gather_all/pallas_call | solution.py:307
  66.6 1.0 select_reduce_fusion.1
  67.6 0.2 fusion.11
  67.8 0.6 select_reduce_fusion
  68.5 0.0 copy-start.1
  68.5 4.6 %multiply_reduce_fusion = (f32[8,128]{1,0:T(8,128)S(1)}, f32[8,128,2048]{2,1,0:T(8,128)S(1)}) fusion(bf16[8,256,2048]{2,1,0:T(8,128)(2,1)} %bitcast.26, f32[8,256]{1,0:T(8,128)S(1)} %fusion.11), kind=kOutput, calls=%fused_computation.2 | convolution fusion | flops 1078197248 | bytes 16789504 | tf_op jit(solution)/shard_map/dot_general | solution.py:590
  73.1 0.0 copy-done.1
  73.2 0.0 copy-start.4
  73.2 0.8 multiply_convert_fusion.1
  74.0 1.2 copy-done.4
  75.2 0.0 copy-start.5
  75.2 4.5 %fusion.1 = f32[1024,896]{1,0:T(8,128)S(1)} fusion(bf16[1024,2048]{1,0:T(8,128)(2,1)S(1)} %bitcast.28, bf16[1,2048,896]{2,1,0:T(8,128)(2,1)S(1)} %copy-done.4), kind=kOutput, calls=%fused_computation.5 | convolution fusion | flops 3758096384 | bytes 11534336 | tf_op jit(solution)/shard_map/dot_general | solution.py:598
  79.7 0.0 copy-done.5
  79.7 0.0 copy-start.6
  79.7 4.8 %multiply_convert_fusion.2 = bf16[1024,896]{1,0:T(8,128)(2,1)S(1)} fusion(f32[1024,896]{1,0:T(8,128)S(1)} %fusion.1, bf16[1024,2048]{1,0:T(8,128)(2,1)S(1)} %bitcast.29, bf16[1,2048,896]{2,1,0:T(8,128)(2,1)S(1)} %copy-done.5), kind=kOutput, calls=%fused_computation.9 | convolution fusion | flops 3763601408 | bytes 13369344 | tf_op jit(solution)/shard_map/dot_general | solution.py:597
  84.5 0.0 copy-done.6
  84.5 4.7 %multiply_convert_fusion = bf16[1024,2048]{1,0:T(8,128)(2,1)S(1)} fusion(bf16[1024,896]{1,0:T(8,128)(2,1)S(1)} %multiply_convert_fusion.2, f32[1024]{0:T(1024)S(1)} %bitcast.30, bf16[1,896,2048]{2,1,0:T(8,128)(2,1)S(1)} %copy-done.6), kind=kOutput, calls=%fused_computation | convolution fusion | flops 3762290688 | bytes 9703424 | tf_op jit(solution)/shard_map/dot_general | solution.py:600
  89.2 5.6 %convolution_convert_fusion = bf16[8,256,2048]{2,1,0:T(8,128)(2,1)} fusion(bf16[8,128,2048]{2,1,0:T(8,128)(2,1)S(1)} %bitcast.27, f32[8,256]{1,0:T(8,128)S(1)} %fusion.11), kind=kOutput, calls=%fused_computation.3 | convolution fusion | flops 1078198272 | bytes 12591104 | tf_op jit(solution)/shard_map/dot_general | solution.py:602
  94.8 63.2 %combine_all.1 = bf16[256,2048]{1,0:T(8,128)(2,1)} custom-call(bf16[2048,2048]{1,0:T(8,128)(2,1)} %bitcast.25, bf16[256,512]{1,0:T(8,128)(2,1)} %fusion.10.own_ref.after_ref), custom_call_target="tpu_custom_call" | custom-call | tf_op jit(solution)/shard_map/combine_all/pallas_call | solution.py:502
  158.0 2.3 %copy.14 = bf16[256,2048]{1,0:T(8,128)(2,1)} copy(bf16[256,2048]{1,0:T(8,128)(2,1)} %combine_all.1) | data formatting | bytes 2097152
  (7 shorter events, 0.0 us)
Async XLA Ops:
  0.0 7.3 %copy-start = (bf16[512,512]{1,0:T(8,128)(2,1)S(1)}, bf16[512,512]{1,0:T(8,128)(2,1)}, u32[]{:S(2)}) copy-start(bf16[512,512]{1,0:T(8,128)(2,1)} %param.12) | copy-start | bytes 1572868
  0.0 6.4 %copy-start.3 = (s32[256,2]{0,1:T(2,128)S(1)}, s32[256,2]{0,1:T(2,128)}, u32[]{:S(2)}) copy-start(s32[256,2]{0,1:T(2,128)} %param.15) | copy-start | bytes 6148
  0.0 6.6 %copy-start.2 = (f32[256,2]{0,1:T(2,128)S(1)}, f32[256,2]{0,1:T(2,128)}, u32[]{:S(2)}) copy-start(f32[256,2]{0,1:T(2,128)} %param.16) | copy-start | bytes 6148
  0.0 7.3 %copy-start.7 = (f32[512]{0:T(512)S(1)}, f32[512]{0:T(512)}, u32[]{:S(2)}) copy-start(f32[512]{0:T(512)} %param.13) | copy-start | bytes 6148
  4.0 3.3 %collective-permute-start = (bf16[16,512]{1,0:T(8,128)(2,1)S(1)}, bf16[16,512]{1,0:T(8,128)(2,1)S(1)}, u32[]{:S(2)}, u32[]{:S(2)}) collective-permute-start(bf16[16,512]{1,0:T(8,128)(2,1)S(1)} %slice.77), channel_id=1, source_target_pairs={{0,4},{4,8},{8,12},{12,16},{16,20},{20,24},{24,28},{1,5},{5,9},{9,... | collective-permute-start | bytes 49160 | tf_op jit(solution)/shard_map/ppermute | solution.py:22
  68.5 4.7 %copy-start.1 = (f32[2048]{0:T(1024)S(1)}, f32[2048]{0:T(1024)}, u32[]{:S(2)}) copy-start(f32[2048]{0:T(1024)} %param.14) | copy-start | bytes 24580
  73.2 2.0 %copy-start.4 = (bf16[1,2048,896]{2,1,0:T(8,128)(2,1)S(1)}, bf16[1,2048,896]{2,1,0:T(8,128)(2,1)}, u32[]{:S(2)}) copy-start(bf16[1,2048,896]{2,1,0:T(8,128)(2,1)} %param.18) | copy-start | bytes 11010052
  75.2 4.5 %copy-start.5 = (bf16[1,2048,896]{2,1,0:T(8,128)(2,1)S(1)}, bf16[1,2048,896]{2,1,0:T(8,128)(2,1)}, u32[]{:S(2)}) copy-start(bf16[1,2048,896]{2,1,0:T(8,128)(2,1)} %param.17) | copy-start | bytes 11010052
  79.7 4.8 %copy-start.6 = (bf16[1,896,2048]{2,1,0:T(8,128)(2,1)S(1)}, bf16[1,896,2048]{2,1,0:T(8,128)(2,1)}, u32[]{:S(2)}) copy-start(bf16[1,896,2048]{2,1,0:T(8,128)(2,1)} %param.19) | copy-start | bytes 11010052

commit v2 on v1

--- a/solution.py
+++ b/solution.py
@@ -185,7 +185,8 @@
 
 
 def gather_kernel(
-    own_ref, meta_ref, out_ref, meta_out, send_sem, recv_sem, p_send, p_recv, m_send, m_recv, l_sem
+    own_ref, meta_ref, result_ref, meta_out,
+    out_ref, send_sem, recv_sem, p_send, p_recv, m_send, m_recv, l_sem, o_sem,
 ):
     place = Place(send_sem, recv_sem)
     rows, cols = own_ref.shape
@@ -197,6 +198,15 @@
     def block(level, core, tile, first=0, count=rows):
         start = pl.multiple_of((level * CORES + core) * rows + first, half)
         return out_ref.at[pl.ds(start, count), pl.ds(pl.multiple_of(tile * cols, cols), cols)]
+
+    def put_out(level, tile, core):
+        start = pl.multiple_of((level * CORES + core) * rows, rows)
+        lanes = pl.ds(pl.multiple_of(tile * cols, cols), cols)
+        return pltpu.make_async_copy(
+            block(level, core, tile),
+            result_ref.at[pl.ds(start, rows), lanes],
+            o_sem.at[level, tile, core],
+        )
 
     def pair_copy(level, tile, core):
         ref = block(level, core, tile)
@@ -249,34 +259,41 @@
         whole(X, level, tp).start()
         whole(Y, level, tp).start()
         pair_copy(level, tp, c).start()
+        put_out(level, tp, c).start()
 
     def second(offset):
         level = z + offset
         whole(X, level, place.tx).wait_recv()
         part(DY, level, place.tx).start()
         pair_copy(level, place.tx, c).start()
+        put_out(level, place.tx, c).start()
         whole(Y, level, place.ty).wait_recv()
         part(DX, level, place.ty).start()
         pair_copy(level, place.ty, c).start()
+        put_out(level, place.ty, c).start()
 
     def third(offset):
         level = z + offset
         part(DY, level, place.td).wait_recv()
         part(DX, level, place.td).wait_recv()
         pair_copy(level, place.td, c).start()
+        put_out(level, place.td, c).start()
 
     order = place.offsets()
-    for step in range(len(order) + 2):
-        if step < len(order):
-            pl.when(place.exists(order[step]))(functools.partial(first, order[step]))
+    stages = ((first, 0), (second, 1), (third, 2))
+    for step in range(place.levels + 2):
+        for stage, lag in stages:
+            for offset in order:
+                if abs(offset) == step - lag:
+                    pl.when(place.exists(offset))(functools.partial(stage, offset))
         if step == 0:
             for hop in range(1, sp_count):
                 meta_copy(hop).start()
-        if 0 <= step - 1 < len(order):
-            pl.when(place.exists(order[step - 1]))(functools.partial(second, order[step - 1]))
-        if 0 <= step - 2 < len(order):
-            pl.when(place.exists(order[step - 2]))(functools.partial(third, order[step - 2]))
-
+
+    pairs = [(level, tile) for level in range(place.levels) for tile in range(tiles)]
+    for level, tile in pairs:
+        pair_copy(level, tile, 1 - c).wait_recv()
+        put_out(level, tile, 1 - c).start()
     for hop in range(1, sp_count):
         meta_copy(hop).wait_send()
         meta_copy(hop).wait_recv()
@@ -294,10 +311,10 @@
 
     for offset in order:
         pl.when(place.exists(offset))(functools.partial(sent, offset))
-    for level in range(place.levels):
-        for tile in range(tiles):
-            pair_copy(level, tile, c).wait_send()
-            pair_copy(level, tile, 1 - c).wait_recv()
+    for level, tile in pairs:
+        pair_copy(level, tile, c).wait_send()
+        put_out(level, tile, c).wait()
+        put_out(level, tile, 1 - c).wait()
 
 
 def gather_all(own, meta, sp_count, tp_count):
@@ -311,8 +328,9 @@
             jax.ShapeDtypeStruct((sp_count,) + meta.shape, meta.dtype),
         ),
         in_specs=[vmem, vmem],
-        out_specs=(vmem, vmem),
+        out_specs=(pl.BlockSpec(memory_space=pl.ANY), vmem),
         scratch_shapes=[
+            pltpu.VMEM((sp_count * rows, tp_count * cols), own.dtype),
             pltpu.SemaphoreType.DMA((6, levels)),
             pltpu.SemaphoreType.DMA((6, levels)),
             pltpu.SemaphoreType.DMA((levels, tp_count)),
@@ -320,6 +338,7 @@
             pltpu.SemaphoreType.DMA((sp_count,)),
             pltpu.SemaphoreType.DMA((sp_count,)),
             pltpu.SemaphoreType.DMA((2,)),
+            pltpu.SemaphoreType.DMA((levels, tp_count, CORES)),
         ],
         compiler_params=pltpu.CompilerParams(collective_id=0, has_side_effects=True),
         name="gather_all",
@@ -328,8 +347,8 @@
 
 def combine_kernel(
     part_ref, after_ref, out_ref,
-    r_pair, s_diag, r_ydiag, r_xdiag, s_x, s_y, r_x, r_y, s_z, r_up, r_down,
-    send_sem, recv_sem, p_send, p_recv,
+    own_part, r_pair, s_diag, r_ydiag, r_xdiag, s_x, s_y, r_x, r_y, s_z, r_up, r_down,
+    send_sem, recv_sem, p_send, p_recv, own_sem,
 ):
     place = Place(send_sem, recv_sem)
     rows, cols = after_ref.shape
@@ -353,11 +372,15 @@
         )
 
     def summed(level, tile, row, count=chunk):
-        start = pl.multiple_of((level * CORES + c) * rows + row, chunk)
+        at = pl.ds(pl.multiple_of(row, chunk), count)
         lanes = pl.ds(pl.multiple_of(tile * cols, cols), cols)
-        mine = part_ref[pl.ds(start, count), lanes].astype(jnp.float32)
-        return mine + r_pair[level, pl.ds(pl.multiple_of(row, chunk), count), lanes].astype(
-            jnp.float32
+        mine = own_part[level, at, lanes].astype(jnp.float32)
+        return mine + r_pair[level, at, lanes].astype(jnp.float32)
+
+    def own_copy(level):
+        start = pl.multiple_of((level * CORES + c) * rows, rows)
+        return pltpu.make_async_copy(
+            part_ref.at[pl.ds(start, rows)], own_part.at[level], own_sem.at[level]
         )
 
     def over(first, last, body):
@@ -383,6 +406,7 @@
     def first(offset):
         level = z + offset
         pair_copy(level).wait_recv()
+        own_copy(level).wait()
 
         def body(row):
             s_diag[level, pl.ds(row, chunk)] = summed(level, place.td, row).astype(jnp.bfloat16)
@@ -451,13 +475,13 @@
     order = place.offsets()[::-1]
     for offset in order:
         pl.when(place.exists(offset))(lambda offset=offset: pair_copy(z + offset).start())
-    for step in range(len(order) + 2):
-        if step < len(order):
-            pl.when(place.exists(order[step]))(functools.partial(first, order[step]))
-        if 0 <= step - 1 < len(order):
-            pl.when(place.exists(order[step - 1]))(functools.partial(second, order[step - 1]))
-        if 0 <= step - 2 < len(order):
-            pl.when(place.exists(order[step - 2]))(functools.partial(third, order[step - 2]))
+        pl.when(place.exists(offset))(lambda offset=offset: own_copy(z + offset).start())
+    stages = ((first, 0), (second, 1), (third, 4))
+    for step in range(len(order) + 4):
+        for stage, lag in stages:
+            if 0 <= step - lag < len(order):
+                offset = order[step - lag]
+                pl.when(place.exists(offset))(functools.partial(stage, offset))
 
     def final(kind, tile):
         start, count = {FX: (0, rows), FY: (0, rows), FDY: (0, half), FDX: (half, half)}[kind]
@@ -502,13 +526,15 @@
     return pl.pallas_call(
         combine_kernel,
         out_shape=jax.ShapeDtypeStruct((rows, tp_count * cols), after.dtype),
-        in_specs=[vmem, vmem],
+        in_specs=[pl.BlockSpec(memory_space=pl.ANY), vmem],
         out_specs=vmem,
         scratch_shapes=[
+            pltpu.VMEM((levels, rows, tp_count * cols), jnp.bfloat16),
             pltpu.VMEM((levels, rows, tp_count * cols), jnp.bfloat16),
             whole, halved, halved, whole, whole, whole, whole, whole, whole, whole,
             pltpu.SemaphoreType.DMA((10, levels)),
             pltpu.SemaphoreType.DMA((10, levels)),
+            pltpu.SemaphoreType.DMA((levels,)),
             pltpu.SemaphoreType.DMA((levels,)),
             pltpu.SemaphoreType.DMA((levels,)),
         ],
@@ -541,7 +567,8 @@
     window = jnp.power(2, group_index + 1)
     stream = residual_in.astype(jnp.float32)
     inverse = lax.rsqrt(jnp.mean(stream * stream, axis=-1, keepdims=True) + EPS)
-    stream_group = lax.dynamic_slice_in_dim(stream, group_index * group_width, group_width, 1)
+    stream_group = lax.dynamic_slice_in_dim(residual_in, group_index * group_width, group_width, 1)
+    stream_group = stream_group.astype(jnp.float32)
     gain_group = lax.dynamic_slice_in_dim(mix_gain, group_index * group_width, group_width, 0)
     normed_group = (stream_group * inverse * gain_group).astype(jnp.bfloat16)
     rim_rows = from_behind(normed_group[tok_count - SPAN :], "sp", 1)
@@ -557,8 +584,8 @@
     mixed = (jnp.dot(pooled, pool_weight, preferred_element_type=jnp.float32) * pool_scale).astype(
         jnp.bfloat16
     )
-    stream_own = lax.dynamic_slice_in_dim(stream, tp_index * col_count, col_count, 1)
-    after_own = (stream_own + mixed.astype(jnp.float32)).astype(jnp.bfloat16)
+    stream_own = lax.dynamic_slice_in_dim(residual_in, tp_index * col_count, col_count, 1)
+    after_own = (stream_own.astype(jnp.float32) + mixed.astype(jnp.float32)).astype(jnp.bfloat16)
 
     meta = jnp.concatenate(
         [

time: 161 us -> 148 us (0.919)
  Pallas kernels: 120 us -> 106 us
    pallas_call x1, Pallas kernels: 57.3 us -> 48.1 us  [gather_all(): pl.pallas_call(gather_kernel, out_shape=(jax.ShapeDtypeStruct((sp_count *...]
    pallas_call x1, Pallas kernels: 63.2 us -> 58.4 us  [combine_all(): pl.pallas_call(combine_kernel, out_shape=jax.ShapeDtypeStruct((rows, tp_c...]
    unnamed x17 -> x11, local copies, waits for them, and re-layouts: 3.58 us -> 3.57 us
  transfers between devices with their start and end apart: 1 -> 1, of which waited for: 0 -> 0; matrix products, arithmetic and copies ran while one was open for 0% -> 1% of each run, Pallas kernels for 0% -> 0%
where the time goes in v2:
time: 148 us
  Pallas kernels  106 us (72%)
  matrix products  27.4 us (19%)
  other arithmetic  7.13 us (5%)
  local copies, waits for them, and re-layouts  4.42 us (3%)
  starting transfers between devices  2.4 us (2%)
    pallas_call x1, Pallas kernels, combine_all(): pl.pallas_call(combine_kernel, out_shape=jax.ShapeDtypeStruct((rows, tp_c...  58.4 us
    pallas_call x1, Pallas kernels, gather_all(): pl.pallas_call(gather_kernel, out_shape=(jax.ShapeDtypeStruct((sp_count *...  48.1 us
    dot_general x1, matrix products, shards(): lax.dot_general(table, term.reshape(sp_count, slots, width), (((1,), (1,)...  5.59 us
    dot_general x1, matrix products, shards(): jnp.dot(flat_rows, gate_weight[0], preferred_element_type=jnp.float32)  4.77 us
    dot_general x1, matrix products, shards(): term = jnp.dot(hidden, down_weight[0], preferred_element_type=jnp.float32)  4.71 us
    dot_general x1, matrix products, shards(): lax.dot_general(table, after_all.reshape(sp_count, tok_count, width), (((...  4.64 us
    dot_general x1, matrix products, shards(): jnp.dot(flat_rows, up_weight[0], preferred_element_type=jnp.float32)  4.49 us
    unnamed x11, local copies, waits for them, and re-layouts  3.57 us
  transfers between devices with their start and end apart: 1, of which 0 were waited for; matrix products, arithmetic and copies ran while one was open for 1% of the time, Pallas kernels for 0%

profile of v2, /device:TPU:0, one launch (start us, length us, event | category | flops | bytes accessed | tf_op | source)
XLA Modules:
  0.0 148.0 jit_solution(1338274280427192576)
XLA Ops:
  0.0 0.0 copy-start
  0.0 1.6 %multiply_reduce_fusion.1 = f32[256]{0:T(256)S(1)} fusion(bf16[256,2048]{1,0:T(8,128)(2,1)} %param.10), kind=kLoop, calls=%fused_computation.10 | loop fusion | flops 1572608 | bytes 1049600 | tf_op jit(solution)/shard_map/reduce_sum | solution.py:569
  1.6 0.8 dynamic_slice.11
  2.4 1.1 multiply_convert_fusion.3
  3.4 2.4 %collective-permute-start = (bf16[16,512]{1,0:T(8,128)(2,1)S(1)}, bf16[16,512]{1,0:T(8,128)(2,1)S(1)}, u32[]{:S(2)}, u32[]{:S(2)}) collective-permute-start(bf16[16,512]{1,0:T(8,128)(2,1)S(1)} %slice.77), channel_id=1, source_target_pairs={{0,4},{4,8},{8,12},{12,16},{16,20},{20,24},{24,28},{1,5},{5,9},{9,... | collective-permute-start | bytes 49160 | tf_op jit(solution)/shard_map/ppermute | solution.py:22
  5.9 0.7 convert_bitcast_fusion
  6.6 0.1 pad.2.clone
  6.7 1.3 maximum_maximum_fusion.meta_ref
  8.0 0.0 collective-permute-done
  8.0 0.1 maximum_convert_fusion
  8.1 0.0 copy-done
  8.1 3.0 %fusion.10.own_ref.after_ref = bf16[256,512]{1,0:T(8,128)(2,1)} fusion(bf16[512,512]{1,0:T(8,128)(2,1)S(1)} %copy-done, f32[512]{0:T(512)} %param.13, bf16[256,2048]{1,0:T(8,128)(2,1)} %param.10, s32[]{:T(128)S(6)} %select_n.166, f32[272,512]{1,0:T(8,128)S(1)} %maximum_convert_fusion, f32[256]{0:T(256)S(1)} %minimum_convert_fusion, pred[]{:T(512)S(6)} %gt.69, ...), kind=kOutput, calls=%fused_computation.15 | convolution fusion | flops 139460608 | bytes 9440276 | tf_op jit(solution)/shard_map/dot_general | solution.py:584
  11.1 48.1 %gather_all.1 = (bf16[2048,2048]{1,0:T(8,128)(2,1)}, f32[8,8,256]{2,1,0:T(8,128)}) custom-call(bf16[256,512]{1,0:T(8,128)(2,1)} %fusion.10.own_ref.after_ref, f32[8,256]{1,0:T(8,128)} %maximum_maximum_fusion.meta_ref), custom_call_target="tpu_custom_call" | custom-call | tf_op jit(solution)/shard_map/gather_all/pallas_call | solution.py:324
  59.1 1.0 select_reduce_fusion.1
  60.1 0.2 fusion.11
  60.3 0.6 select_reduce_fusion
  61.0 0.0 copy-start.1
  61.0 4.6 %multiply_reduce_fusion = (f32[8,128]{1,0:T(8,128)S(1)}, f32[8,128,2048]{2,1,0:T(8,128)S(1)}) fusion(bf16[8,256,2048]{2,1,0:T(8,128)(2,1)} %bitcast.26, f32[8,256]{1,0:T(8,128)S(1)} %fusion.11), kind=kOutput, calls=%fused_computation.2 | convolution fusion | flops 1078197248 | bytes 16789504 | tf_op jit(solution)/shard_map/dot_general | solution.py:617
  65.6 0.0 copy-done.1
  65.6 0.0 copy-start.2
  65.7 0.8 multiply_convert_fusion.1
  66.4 1.2 copy-done.2
  67.7 0.0 copy-start.3
  67.7 4.5 %fusion.1 = f32[1024,896]{1,0:T(8,128)S(1)} fusion(bf16[1024,2048]{1,0:T(8,128)(2,1)S(1)} %bitcast.28, bf16[1,2048,896]{2,1,0:T(8,128)(2,1)S(1)} %copy-done.2), kind=kOutput, calls=%fused_computation.5 | convolution fusion | flops 3758096384 | bytes 11534336 | tf_op jit(solution)/shard_map/dot_general | solution.py:625
  72.2 0.0 copy-done.3
  72.2 0.0 copy-start.4
  72.2 4.8 %multiply_convert_fusion.2 = bf16[1024,896]{1,0:T(8,128)(2,1)S(1)} fusion(f32[1024,896]{1,0:T(8,128)S(1)} %fusion.1, bf16[1024,2048]{1,0:T(8,128)(2,1)S(1)} %bitcast.29, bf16[1,2048,896]{2,1,0:T(8,128)(2,1)S(1)} %copy-done.3), kind=kOutput, calls=%fused_computation.9 | convolution fusion | flops 3763601408 | bytes 13369344 | tf_op jit(solution)/shard_map/dot_general | solution.py:624
  77.0 0.0 copy-done.4
  77.0 4.7 %multiply_convert_fusion = bf16[1024,2048]{1,0:T(8,128)(2,1)S(1)} fusion(bf16[1024,896]{1,0:T(8,128)(2,1)S(1)} %multiply_convert_fusion.2, f32[1024]{0:T(1024)S(1)} %bitcast.30, bf16[1,896,2048]{2,1,0:T(8,128)(2,1)S(1)} %copy-done.4), kind=kOutput, calls=%fused_computation | convolution fusion | flops 3762290688 | bytes 9703424 | tf_op jit(solution)/shard_map/dot_general | solution.py:627
  81.7 5.6 %convolution_convert_fusion = bf16[8,256,2048]{2,1,0:T(8,128)(2,1)} fusion(bf16[8,128,2048]{2,1,0:T(8,128)(2,1)S(1)} %bitcast.27, f32[8,256]{1,0:T(8,128)S(1)} %fusion.11), kind=kOutput, calls=%fused_computation.3 | convolution fusion | flops 1078198272 | bytes 12591104 | tf_op jit(solution)/shard_map/dot_general | solution.py:629
  87.3 58.4 %combine_all.1 = bf16[256,2048]{1,0:T(8,128)(2,1)} custom-call(bf16[2048,2048]{1,0:T(8,128)(2,1)} %bitcast.25, bf16[256,512]{1,0:T(8,128)(2,1)} %fusion.10.own_ref.after_ref), custom_call_target="tpu_custom_call" | custom-call | tf_op jit(solution)/shard_map/combine_all/pallas_call | solution.py:526
  145.7 2.3 %copy.14 = bf16[256,2048]{1,0:T(8,128)(2,1)} copy(bf16[256,2048]{1,0:T(8,128)(2,1)} %combine_all.1) | data formatting | bytes 2097152
  (6 shorter events, 0.0 us)
Async XLA Ops:
  0.0 8.1 %copy-start = (bf16[512,512]{1,0:T(8,128)(2,1)S(1)}, bf16[512,512]{1,0:T(8,128)(2,1)}, u32[]{:S(2)}) copy-start(bf16[512,512]{1,0:T(8,128)(2,1)} %param.12) | copy-start | bytes 1572868
  3.4 4.6 %collective-permute-start = (bf16[16,512]{1,0:T(8,128)(2,1)S(1)}, bf16[16,512]{1,0:T(8,128)(2,1)S(1)}, u32[]{:S(2)}, u32[]{:S(2)}) collective-permute-start(bf16[16,512]{1,0:T(8,128)(2,1)S(1)} %slice.77), channel_id=1, source_target_pairs={{0,4},{4,8},{8,12},{12,16},{16,20},{20,24},{24,28},{1,5},{5,9},{9,... | collective-permute-start | bytes 49160 | tf_op jit(solution)/shard_map/ppermute | solution.py:22
  61.0 4.7 %copy-start.1 = (f32[2048]{0:T(1024)S(1)}, f32[2048]{0:T(1024)}, u32[]{:S(2)}) copy-start(f32[2048]{0:T(1024)} %param.14) | copy-start | bytes 24580
  65.6 2.0 %copy-start.2 = (bf16[1,2048,896]{2,1,0:T(8,128)(2,1)S(1)}, bf16[1,2048,896]{2,1,0:T(8,128)(2,1)}, u32[]{:S(2)}) copy-start(bf16[1,2048,896]{2,1,0:T(8,128)(2,1)} %param.18) | copy-start | bytes 11010052
  67.7 4.5 %copy-start.3 = (bf16[1,2048,896]{2,1,0:T(8,128)(2,1)S(1)}, bf16[1,2048,896]{2,1,0:T(8,128)(2,1)}, u32[]{:S(2)}) copy-start(bf16[1,2048,896]{2,1,0:T(8,128)(2,1)} %param.17) | copy-start | bytes 11010052
  72.2 4.8 %copy-start.4 = (bf16[1,896,2048]{2,1,0:T(8,128)(2,1)S(1)}, bf16[1,896,2048]{2,1,0:T(8,128)(2,1)}, u32[]{:S(2)}) copy-start(bf16[1,896,2048]{2,1,0:T(8,128)(2,1)} %param.19) | copy-start | bytes 11010052
